TPU v7x, 256 devices: a whole 4x4x8 slice. The times are simulated.
256 devices in a mesh: dp: 4 (over x), kv: 32 (over z, y), tp: 2 (over core).
Axes of the slice: x: 4, y: 4, z: 8, core: 2. Of those that a mesh axis runs over, the one named last changes fastest.
Arguments:
- tokens: bfloat16 [64, 16, 4096], P('dp', None, 'kv'), may hold values from -64 to 64
- in_gain: bfloat16 [4096], P('kv'), may hold values from 0.099609375 to 1.8984375
- query_weight: bfloat16 [4096, 4096], P('kv', 'tp'), may hold values from -0.125 to 0.125
- key_weight: bfloat16 [4096, 4096], P('kv', 'tp'), may hold values from -0.125 to 0.125
- value_weight: bfloat16 [4096, 4096], P('kv', 'tp'), may hold values from -0.09375 to 0.09375
- out_weight: bfloat16 [4096, 4096], P('tp', 'kv'), may hold values from -0.1875 to 0.1875
- lambdas: float32 [16], P('tp'), may hold values from 0.3 to 0.8
- sub_gain: bfloat16 [256], replicated, may hold values from 0.099609375 to 1.8984375
- key_cache: bfloat16 [64, 1024, 16, 2, 128], P('dp', 'kv', 'tp'), may hold values from -248 to 248
- value_cache: bfloat16 [64, 1024, 16, 256], P('dp', 'kv', 'tp'), may hold values from -6 to 6
- cache_len: int32 [64], P('dp'), may hold values from 512 to 992
- accepted: int32 [64], P('dp'), may hold values from 0 to 16
- parents: int32 [64, 16], P('dp'), may hold values from -1 to 14, as said below
Outputs:
- output: bfloat16 [64, 16, 4096], P('dp', None, ('kv', 'tp'))
- key_cache_out: bfloat16 [64, 1024, 16, 2, 128], P('dp', 'kv', 'tp')
- value_cache_out: bfloat16 [64, 1024, 16, 256], P('dp', 'kv', 'tp')
Inputs may be any that keep to these rules, and one draw needn't show every extreme that they name: `parents`: each proposal's parent is -1 (the text already in the cache) or one of the three proposals just before it; the last proposal's parent is the one just before it. Positions below cache_len plus accepted hold a sequence's text; the later ones are stale.
All inputs are finite; a program needn't handle non-finite values.
Results may differ from a plain program's by a relative error of at most 0.019.
The roundings to bfloat16 on the way count: a program that leaves them out, or rounds other values in their place, can miss the bound.
Values may be sent and summed in bfloat16 or wider, within the bound.
No kernel may reach another device: no remote copies, remote signals or barrier semaphores. Data moves between devices by JAX's collectives and lax.ppermute only.
A program may use at most 64 MiB of HBM per device.

v0:
```python
import math

import jax
import jax.numpy as jnp
from jax import lax
from jax.sharding import Mesh
from jax.sharding import PartitionSpec as P

D = 4096
KV = ("kv_0", "kv_1")
KV_TP = ("kv_0", "kv_1", "tp")


LAMBDA_SCALE = 0.2 + 0.6 * math.exp(-0.6)
NEG_FILL = -1e30


def sent_to_all(value, axis):
    size = lax.axis_size(axis)
    return lax.all_to_all(
        jnp.broadcast_to(value[None], (size, *value.shape)), axis, 0, 0, tiled=True
    )


def over_copies(value, axis):
    return sent_to_all(value, axis).sum(axis=0)


def gather_axes(value, axes, dim):
    for axis in reversed(axes):
        value = lax.all_gather(value, axis, axis=dim, tiled=True)
    return value


def rows_first(arrays, axis, dims):
    turned = [jnp.moveaxis(a, dim, 0) for a, dim in zip(arrays, dims)]
    widths = [t[0].size for t in turned]
    both = jnp.concatenate([t.reshape(-1, w) for t, w in zip(turned, widths)], axis=1)
    filled = lax.all_gather(both, axis, axis=0, tiled=True)
    pieces = jnp.split(filled, [sum(widths[:k]) for k in range(1, len(widths))], axis=1)
    return tuple(
        (
            jnp.moveaxis(b.reshape(-1, *t.shape[1:]), 0, dim)
            for b, t, dim in zip(pieces, turned, dims)
        )
    )


def all_in_one(value, axis):
    leaves = jax.tree.leaves(value)
    order = sorted(range(len(leaves)), key=lambda k: -leaves[k].size)
    width = (1, *leaves[order[0]].shape)[-1]
    lines = [
        jnp.pad(leaves[k].reshape(-1), (0, -leaves[k].size % width)).reshape(-1, width)
        for k in order
    ]
    both, at, found = (lax.all_gather(jnp.concatenate(lines), axis), 0, {})
    for k, line in zip(order, lines):
        share = both[:, at : at + len(line)].reshape(len(both), -1)
        found[k] = share[:, : leaves[k].size].reshape(-1, *leaves[k].shape)
        at += len(line)
    numbers = iter(range(len(leaves)))
    return jax.tree.map(lambda _: found[next(numbers)], value)


def merged_by_axis(value, axes, combine):
    for axis in axes:
        pieces = all_in_one(value, axis)
        value = jax.tree.map(lambda part: part[0], pieces)
        for k in range(1, lax.axis_size(axis)):
            value = combine(value, jax.tree.map(lambda part: part[k], pieces))
    return value


def by_axis(value, axes):
    for axis in axes:
        value = lax.psum(value, axis)
    return value


def split_up(value, dim, size):
    lengths = value.shape
    pieces = value.reshape(*lengths[:dim], size, lengths[dim] // size, *lengths[dim + 1 :])
    return jnp.moveaxis(pieces, dim, 0)


def sent_and_summed(value, axis, dim):
    pieces = split_up(value, dim, lax.axis_size(axis))
    arrived = lax.all_to_all(pieces, axis, split_axis=0, concat_axis=0, tiled=True)
    return arrived.astype(jnp.float32).sum(axis=0)


def visible_links(parents):
    number = parents.shape[-1]
    identity = jnp.eye(number, dtype=jnp.float32)
    parent_links = (parents[..., :, None] == jnp.arange(number, dtype=jnp.int32)[None, :]).astype(
        jnp.float32
    )

    def extend(repeat, reached):
        return jnp.maximum(
            identity,
            jnp.einsum("bij,bjk->bik", parent_links, reached, precision=lax.Precision.HIGHEST),
        )

    reached = lax.fori_loop(0, number, extend, jnp.broadcast_to(identity, parent_links.shape))
    depths = (jnp.sum(reached, axis=-1) - 1.0).astype(jnp.int32)
    return (reached > 0.5, depths)


def merge_stats(former, latter):
    highest = jnp.maximum(former[0], latter[0])
    totals = former[1] * jnp.exp(former[0] - highest) + latter[1] * jnp.exp(latter[0] - highest)
    return (highest, totals)


def per_device(
    tokens,
    in_gain,
    query_weight,
    key_weight,
    value_weight,
    out_weight,
    lambdas,
    sub_gain,
    key_cache,
    value_cache,
    cache_len,
    accepted,
    parents,
):
    seq_count, prop_count, width_part = tokens.shape
    heads_here = lambdas.shape[0]
    span_here = key_cache.shape[1]
    head_dim = key_cache.shape[-1]
    half_dim = head_dim // 2
    row_count = seq_count * prop_count
    tokens_wide = tokens.astype(jnp.float32)
    squares = over_copies(jnp.sum(tokens_wide * tokens_wide, axis=-1), KV)
    row_scale = lax.rsqrt(squares.reshape(row_count) / D + 1e-06)
    normed = (
        (tokens_wide * in_gain.astype(jnp.float32))
        .astype(jnp.bfloat16)
        .reshape(row_count, width_part)
    )
    starts = cache_len + accepted
    visible, depths = visible_links(parents)
    positions = (starts[:, None] + depths).reshape(row_count)

    def pair_order(weight):
        rows_here = weight.shape[0]
        return (
            weight.reshape(rows_here, 2 * heads_here, 2, half_dim)
            .transpose(0, 1, 3, 2)
            .reshape(rows_here, -1)
        )

    cols_q, cols_k, cols_v = (
        lax.all_to_all(pair_order(query_weight), KV, split_axis=1, concat_axis=0, tiled=True),
        lax.all_to_all(pair_order(key_weight), KV, split_axis=1, concat_axis=0, tiled=True),
        lax.all_to_all(value_weight, KV, split_axis=1, concat_axis=0, tiled=True),
    )
    all_normed = gather_axes(normed, KV, 1)
    pair_count = cols_q.shape[1] // 2
    first_pair = lax.axis_index(KV) * pair_count
    pair_slot = (first_pair + jnp.arange(pair_count, dtype=jnp.int32)) % half_dim
    frequency = 10000.0 ** (-pair_slot.astype(jnp.float32) / half_dim)
    angles = positions.astype(jnp.float32)[:, None] * frequency[None, :]
    cosine = jnp.cos(angles)
    sine_part = jnp.sin(angles)

    def turned(weight):
        product = (
            jnp.dot(all_normed, weight, preferred_element_type=jnp.float32) * row_scale[:, None]
        )
        pairs = product.reshape(row_count, pair_count, 2)
        lower_half = pairs[..., 0]
        upper_half = pairs[..., 1]
        result = jnp.stack(
            [
                lower_half * cosine - upper_half * sine_part,
                upper_half * cosine + lower_half * sine_part,
            ],
            axis=-1,
        )
        return result.reshape(row_count, 2 * pair_count).astype(jnp.bfloat16)

    own_q = turned(cols_q)
    own_k = turned(cols_k)
    own_v = (
        jnp.dot(all_normed, cols_v, preferred_element_type=jnp.float32) * row_scale[:, None]
    ).astype(jnp.bfloat16)
    got_q, got_k, new_values = rows_first((own_q, own_k, own_v), KV, (1, 1, 1))

    def head_order(rows):
        return (
            rows.reshape(row_count, 2 * heads_here, half_dim, 2)
            .transpose(0, 1, 3, 2)
            .reshape(row_count, -1)
        )

    queries = head_order(got_q)
    new_keys = head_order(got_k)
    query_blocks = queries.reshape(seq_count, prop_count, heads_here, 2, head_dim)
    key_blocks = new_keys.reshape(seq_count, prop_count, heads_here, 2, head_dim)
    value_blocks = new_values.reshape(seq_count, prop_count, heads_here, 2 * head_dim)
    offset = lax.axis_index(KV) * span_here
    slot_index = starts[:, None] + jnp.arange(prop_count, dtype=jnp.int32)[None, :] - offset
    slot_index = jnp.where((slot_index >= 0) & (slot_index < span_here), slot_index, span_here)
    seq_index = jnp.broadcast_to(jnp.arange(seq_count, dtype=jnp.int32)[:, None], slot_index.shape)
    key_out = key_cache.at[seq_index, slot_index].set(key_blocks, mode="drop")
    value_out = value_cache.at[seq_index, slot_index].set(value_blocks, mode="drop")
    inverse_root = head_dim ** (-0.5)
    cache_scores = (
        jnp.einsum(
            "bqhmd,bthmd->bhmqt", query_blocks, key_cache, preferred_element_type=jnp.float32
        )
        * inverse_root
    )
    live_mask = (offset + jnp.arange(span_here, dtype=jnp.int32))[None, :] < starts[:, None]
    live_mask = live_mask[:, None, None, None, :]
    cache_scores = jnp.where(live_mask, cache_scores, NEG_FILL)
    local_peak = jnp.max(cache_scores, axis=-1)
    local_total = jnp.sum(
        jnp.where(live_mask, jnp.exp(cache_scores - local_peak[..., None]), 0.0), axis=-1
    )
    cache_peak, cache_total = merged_by_axis((local_peak, local_total), KV, merge_stats)
    own_scores = (
        jnp.einsum(
            "bqhmd,bjhmd->bhmqj", query_blocks, key_blocks, preferred_element_type=jnp.float32
        )
        * inverse_root
    )
    seen_mask = visible[:, None, None]
    own_scores = jnp.where(seen_mask, own_scores, NEG_FILL)
    own_peak = jnp.max(own_scores, axis=-1)
    own_total = jnp.sum(
        jnp.where(seen_mask, jnp.exp(own_scores - own_peak[..., None]), 0.0), axis=-1
    )
    peak_all, totals = merge_stats((cache_peak, cache_total), (own_peak, own_total))
    lam_mix = lambdas[None, :, None, None]

    def weights_of(scores, alive):
        probs = jnp.where(alive, jnp.exp(scores - peak_all[..., None]), 0.0) / totals[..., None]
        return (probs[:, :, 0] - lam_mix * probs[:, :, 1]).astype(jnp.bfloat16)

    cache_weight = weights_of(cache_scores, live_mask)
    partial_value = jnp.einsum(
        "bhqt,bthe->bqhe", cache_weight, value_cache, preferred_element_type=jnp.float32
    )
    summed = by_axis(partial_value.astype(jnp.bfloat16), KV).astype(jnp.float32)
    own_weight = weights_of(own_scores, seen_mask)
    attended = summed + jnp.einsum(
        "bhqj,bjhe->bqhe", own_weight, value_blocks, preferred_element_type=jnp.float32
    )
    mixed_out = attended * lax.rsqrt(jnp.mean(attended * attended, axis=-1, keepdims=True) + 1e-05)
    mixed_out = (mixed_out * sub_gain.astype(jnp.float32) * LAMBDA_SCALE).astype(jnp.bfloat16)
    mixed_out = mixed_out.reshape(row_count, heads_here * 2 * head_dim)
    product = jnp.dot(mixed_out, out_weight, preferred_element_type=jnp.float32).reshape(
        seq_count, prop_count, -1
    )
    output = sent_and_summed(product.astype(jnp.bfloat16), "tp", 2).astype(jnp.bfloat16)
    return (output, key_out, value_out)


def solution(mesh):
    torus = Mesh(
        mesh.devices.reshape(mesh.shape["dp"], 8, 4, mesh.shape["tp"]), ("dp", "kv_0", "kv_1", "tp")
    )
    placed = (
        P("dp", None, KV),
        P(KV),
        P(KV, "tp"),
        P(KV, "tp"),
        P(KV, "tp"),
        P("tp", KV),
        P("tp"),
        P(),
        P("dp", KV, "tp", None, None),
        P("dp", KV, "tp", None),
        P("dp"),
        P("dp"),
        P("dp", None),
    )
    return jax.shard_map(
        per_device,
        mesh=torus,
        in_specs=placed,
        out_specs=(P("dp", None, KV_TP), P("dp", KV, "tp", None, None), P("dp", KV, "tp", None)),
        check_vma=False,
    )
```

profile of v0, /device:TPU:1, one launch (start us, length us, event | category | flops | bytes accessed | tf_op | source)
XLA Modules:
  0.0 426.4 jit_solution(6596932507538783749)
XLA Ops:
  7.2 4.6 %copy.611 = bf16[16,32,8,2,128]{4,3,2,1,0:T(2,128)(2,1)} copy(bf16[16,32,8,2,128]{4,3,2,1,0:T(2,128)(2,1)} %param.23) | data formatting | bytes 4194304
  14.1 12.0 %all-to-all-start.1 = ((f32[32,1,256]{2,1,0:T(1,128)}), f32[32,1,256]{2,1,0:T(1,128)S(1)}, u32[]{:S(2)}, u32[]{:S(2)}) async-start(f32[32,1,256]{2,1,0:T(1,128)} %reshape.538), calls=%async_computation.1 | async-start | bytes 65536 | tf_op jit(solution)/shard_map/all_to_all | solution.py:20
  27.7 7.1 %all-to-all-done.1 = f32[32,1,256]{2,1,0:T(1,128)S(1)} async-done(((f32[32,1,256]{2,1,0:T(1,128)}), f32[32,1,256]{2,1,0:T(1,128)S(1)}, u32[]{:S(2)}, u32[]{:S(2)}) %all-to-all-start.1) | async-done | bytes 32800 | tf_op jit(solution)/shard_map/all_to_all | solution.py:20
  34.8 3.9 all-to-all-start
  38.8 12.7 %all_gather.21 = bf16[256,512]{1,0:T(8,128)(2,1)} all-gather(bf16[256,128]{1,0:T(8,128)(2,1)S(1)} %bitcast.359), channel_id=1, replica_groups=mesh['dp'=4,'kv_0'=8,'kv_1'=4,'tp'=2] {'kv_1'}, dimensions={1}, use_global_device_ids=true | all-gather | bytes 327680 | tf_op jit(solution)/shard_map/all_gather | solution.py:31
  53.6 8.8 %all-to-all-start.2 = ((bf16[128,32,64]{0,2,1:T(8,128)(2,1)}), bf16[128,32,64]{0,2,1:T(8,128)(2,1)}, u32[]{:S(2)}, u32[]{:S(2)}) async-start(bf16[128,32,64]{0,2,1:T(8,128)(2,1)} %bitcast.8), calls=%async_computation.2 | async-start | bytes 1048576 | tf_op jit(solution)/shard_map/all_to_all | solution.py:160
  62.5 5.8 %while.11 = (s32[]{:T(128)}, f32[16,16,16]{2,1,0:T(8,128)S(1)}, s32[16,16]{1,0:T(8,128)S(1)}, s32[]{:T(128)}) while((s32[]{:T(128)}, f32[16,16,16]{2,1,0:T(8,128)S(1)}, s32[16,16]{1,0:T(8,128)S(1)}, s32[]{:T(128)}) %tuple.80), condition=%wide.region_3.0_spmd.clone, body=%wide.region_2.0_spmd.clone.sunk | while | flops 799234 | bytes 68661 | solution.py:106
  71.1 27.8 %all-gather.5.cloned.1.call-done = bf16[256,4096]{1,0:T(8,128)(2,1)} async-done(((bf16[256,512]{1,0:T(8,128)(2,1)}), bf16[256,4096]{1,0:T(8,128)(2,1)}) %all-gather.5.cloned.1.call-update) | async-done | bytes 2097168 | tf_op jit(solution)/shard_map/all_gather | solution.py:31
  98.8 2.5 convolution_multiply_fusion.2
  101.4 6.8 %all-to-all-start.3 = ((bf16[128,32,64]{0,2,1:T(8,128)(2,1)}), bf16[128,32,64]{0,2,1:T(8,128)(2,1)S(1)}, u32[]{:S(2)}, u32[]{:S(2)}) async-start(bf16[128,32,64]{0,2,1:T(8,128)(2,1)} %bitcast.333), calls=%async_computation.3 | async-start | bytes 1048576 | tf_op jit(solution)/shard_map/all_to_all | solution.py:161
  108.2 1.8 convolution_multiply_fusion.1
  110.6 10.7 %all-to-all-done.3 = bf16[128,32,64]{0,2,1:T(8,128)(2,1)S(1)} async-done(((bf16[128,32,64]{0,2,1:T(8,128)(2,1)}), bf16[128,32,64]{0,2,1:T(8,128)(2,1)S(1)}, u32[]{:S(2)}, u32[]{:S(2)}) %all-to-all-start.3) | async-done | bytes 524320 | tf_op jit(solution)/shard_map/all_to_all | solution.py:161
  123.1 76.4 %all-gather.7.cloned.1.call-done = bf16[2048,768]{1,0:T(8,128)(2,1)} async-done(((bf16[64,768]{1,0:T(8,128)(2,1)}), bf16[2048,768]{1,0:T(8,128)(2,1)}) %all-gather.7.cloned.1.call-update) | async-done | bytes 3145744 | tf_op jit(solution)/shard_map/all_gather | solution.py:39
  199.5 3.7 fusion.103
  204.4 4.9 %copy.326 = bf16[256,16,64,2]{2,3,0,1:T(2,128)(2,1)S(1)} copy(bf16[256,16,64,2]{0,3,2,1:T(2,128)(2,1)} %reshape.515) | data formatting | bytes 2097152 | tf_op jit(solution)/shard_map/reshape | solution.py:197
  209.3 1.8 reshape_reshape.4
  211.1 3.3 fusion.110
  217.3 19.1 %all-gather = f32[4096,16]{0,1:T(8,128)S(1)} all-gather(f32[512,16]{0,1:T(8,128)S(1)} %pad_maximum_fusion.3), channel_id=2, replica_groups=mesh['dp'=4,'kv_0'=8,'kv_1'=4,'tp'=2] {'kv_0'}, dimensions={0}, use_global_device_ids=true | all-gather | bytes 294912 | tf_op jit(solution)/shard_map/all_gather | solution.py:57
  237.0 9.1 %all-gather.1 = f32[2048,16]{0,1:T(8,128)S(1)} all-gather(f32[512,16]{0,1:T(8,128)S(1)} %pad_maximum_fusion.4), channel_id=3, replica_groups=mesh['dp'=4,'kv_0'=8,'kv_1'=4,'tp'=2] {'kv_1'}, dimensions={0}, use_global_device_ids=true | all-gather | bytes 163840 | tf_op jit(solution)/shard_map/all_gather | solution.py:57
  249.7 3.9 copy.353
  253.5 4.9 %reshape_reshape.5 = bf16[16,16,8,2,128]{4,1,0,3,2:T(8,128)(2,1)} reshape(bf16[256,16,2,64]{3,2,0,1:T(2,128)(2,1)} %copy.353) | data formatting | bytes 2097152 | tf_op jit(solution)/shard_map/reshape;reshape | solution.py:205
  258.4 2.0 fusion.109
  266.2 81.4 %all-reduce.3.cloned.1.call-done = bf16[16,16,8,256]{3,1,2,0:T(8,128)(2,1)} async-done(((bf16[16,16,8,256]{3,1,2,0:T(8,128)(2,1)}), bf16[16,16,8,256]{3,1,2,0:T(8,128)(2,1)}) %all-reduce.3.cloned.1.call-update) | async-done | bytes 1048592 | tf_op jit(solution)/shard_map/psum | solution.py:77
  347.8 2.3 copy.362
  350.0 2.5 copy.399
  352.6 3.7 copy.368
  356.2 2.6 copy.369
  358.8 29.1 %scatter_fusion = bf16[16,32,8,2,128]{4,3,2,1,0:T(2,128)(2,1)} fusion(bf16[16,32,8,2,128]{4,3,2,1,0:T(2,128)(2,1)} %copy.611, s32[256]{0:T(256)S(1)} %reshape.521, bf16[256,8,2,128]{3,2,1,0:T(2,128)(2,1)} %copy.368), kind=kCustom, calls=%fused_computation | custom fusion | bytes 3147776 | tf_op jit(solution)/shard_map/scatter | solution.py:211
  388.0 14.0 %scatter_fusion.1 = bf16[16,32,8,256]{3,2,1,0:T(8,128)(2,1)S(1)} fusion(bf16[16,32,8,256]{3,2,1,0:T(8,128)(2,1)S(1)} %copy-done.2, s32[256]{0:T(256)S(1)} %reshape.521, bf16[256,8,256]{2,1,0:T(8,128)(2,1)} %copy.369), kind=kCustom, calls=%fused_computation.1 | custom fusion | bytes 3147776 | tf_op jit(solution)/shard_map/scatter | solution.py:212
  402.0 4.3 %select_divide_fusion = f32[16,8,2,16,16]{3,4,2,1,0:T(8,128)} fusion(f32[16,8,2,16,16]{3,4,2,1,0:T(8,128)} %copy-done.7, f32[16,8,2,16]{3,2,1,0:T(2,128)S(1)} %bitcast.337, f32[16,8,2,16]{3,2,1,0:T(2,128)S(1)} %bitcast.339, pred[16,16,16]{1,2,0:T(8,128)(4,1)S(1)} %copy-done.18), kind=kLoop, calls=%fused_computation.17 | loop fusion | flops 196608 | bytes 561152 | tf_op jit(solution)/shard_map/div | solution.py:244
  406.3 2.9 multiply_reduce_fusion
  410.5 8.6 %all_to_all.67 = bf16[2,2,8192]{2,1,0:T(2,128)(2,1)S(1)} all-to-all(bf16[2,2,8192]{2,1,0:T(2,128)(2,1)S(1)} %reshape.540), channel_id=1, replica_groups=mesh['dp'=4,'kv_0'=8,'kv_1'=4,'tp'=2] {'tp'}, dimensions={0} | all-to-all | bytes 131072 | tf_op jit(solution)/shard_map/all_to_all | solution.py:89
  (188 shorter events, 32.4 us)
Async XLA Ops:
  7.2 402.6 %copy-start = (bf16[2048,128]{1,0:T(8,128)(2,1)S(1)}, bf16[2048,128]{1,0:T(8,128)(2,1)}, u32[]{:S(2)}) copy-start(bf16[2048,128]{1,0:T(8,128)(2,1)} %param.20) | copy-start | bytes 1572868
  7.2 4.6 %copy-start.9 = (bf16[16,32,8,256]{3,2,1,0:T(8,128)(2,1)S(1)}, bf16[16,32,8,256]{3,2,1,0:T(8,128)(2,1)}, u32[]{:S(2)}) copy-start(bf16[16,32,8,256]{3,2,1,0:T(8,128)(2,1)} %param.24) | copy-start | bytes 6291460
  11.8 1.4 copy-start.22
  11.8 1.4 copy-start.20
  11.8 14.3 %copy-start.11 = (bf16[128,2048]{1,0:T(8,128)(2,1)S(1)}, bf16[128,2048]{1,0:T(8,128)(2,1)}, u32[]{:S(2)}) copy-start(bf16[128,2048]{1,0:T(8,128)(2,1)} %param.17) | copy-start | bytes 1572868
  13.3 38.2 %copy-start.12 = (bf16[128,2048]{1,0:T(8,128)(2,1)S(1)}, bf16[128,2048]{1,0:T(8,128)(2,1)}, u32[]{:S(2)}) copy-start(bf16[128,2048]{1,0:T(8,128)(2,1)} %param.18) | copy-start | bytes 1572868
  14.1 20.7 %all-to-all-start.1 = ((f32[32,1,256]{2,1,0:T(1,128)}), f32[32,1,256]{2,1,0:T(1,128)S(1)}, u32[]{:S(2)}, u32[]{:S(2)}) async-start(f32[32,1,256]{2,1,0:T(1,128)} %reshape.538), calls=%async_computation.1 | async-start | bytes 65536 | tf_op jit(solution)/shard_map/all_to_all | solution.py:20
  34.8 18.8 %all-to-all-start = ((bf16[128,32,64]{0,2,1:T(8,128)(2,1)}), bf16[128,32,64]{0,2,1:T(8,128)(2,1)S(1)}, u32[]{:S(2)}, u32[]{:S(2)}) async-start(bf16[128,32,64]{0,2,1:T(8,128)(2,1)} %bitcast.3), calls=%async_computation | async-start | bytes 1048576 | tf_op jit(solution)/shard_map/all_to_all | solution.py:159
  38.7 23.7 %copy-start.19 = (s32[16,16]{1,0:T(8,128)S(1)}, s32[16,16]{1,0:T(8,128)}, u32[]{:S(2)}) copy-start(s32[16,16]{1,0:T(8,128)} %param.27) | copy-start | bytes 3076
  38.7 60.1 %all-gather.5.cloned.1.call-start = ((), (), s32[]{:S(2)}) async-start(), calls=%async_computation.5 | async-start | bytes 2359296 | tf_op jit(solution)/shard_map/all_gather | solution.py:31
  53.1 15.1 %copy-start.23 = (s32[16]{0:T(128)S(1)}, s32[16]{0:T(128)}, u32[]{:S(2)}) copy-start(s32[16]{0:T(128)} %param.25) | copy-start | bytes 196
  53.1 15.1 %copy-start.24 = (s32[16]{0:T(128)S(1)}, s32[16]{0:T(128)}, u32[]{:S(2)}) copy-start(s32[16]{0:T(128)} %param.26) | copy-start | bytes 196
  53.6 14.9 %copy-start.13 = (bf16[128,2048]{1,0:T(8,128)(2,1)S(1)}, bf16[128,2048]{1,0:T(8,128)(2,1)}, u32[]{:S(2)}) copy-start(bf16[128,2048]{1,0:T(8,128)(2,1)} %param.19) | copy-start | bytes 1572868
  53.6 47.7 %all-to-all-start.2 = ((bf16[128,32,64]{0,2,1:T(8,128)(2,1)}), bf16[128,32,64]{0,2,1:T(8,128)(2,1)}, u32[]{:S(2)}, u32[]{:S(2)}) async-start(bf16[128,32,64]{0,2,1:T(8,128)(2,1)} %bitcast.8), calls=%async_computation.2 | async-start | bytes 1048576 | tf_op jit(solution)/shard_map/all_to_all | solution.py:160
  98.8 9.4 %copy-start.1 = (bf16[256,4096]{1,0:T(8,128)(2,1)S(1)}, bf16[256,4096]{1,0:T(8,128)(2,1)}, u32[]{:S(2)}) copy-start(bf16[256,4096]{1,0:T(8,128)(2,1)} %all-gather.5.cloned.1.call-done) | copy-start | bytes 6291460
  101.4 19.9 %all-to-all-start.3 = ((bf16[128,32,64]{0,2,1:T(8,128)(2,1)}), bf16[128,32,64]{0,2,1:T(8,128)(2,1)S(1)}, u32[]{:S(2)}, u32[]{:S(2)}) async-start(bf16[128,32,64]{0,2,1:T(8,128)(2,1)} %bitcast.333), calls=%async_computation.3 | async-start | bytes 1048576 | tf_op jit(solution)/shard_map/all_to_all | solution.py:161
  108.2 91.3 %all-gather.7.cloned.1.call-start = ((), (), s32[]{:S(2)}) async-start(), calls=%async_computation.6 | async-start | bytes 3244032 | tf_op jit(solution)/shard_map/all_gather | solution.py:39
  122.8 224.8 %all-reduce.3.cloned.1.call-start = ((), (), s32[]{:S(2)}) async-start(), calls=%async_computation.7 | async-start | bytes 2097152 | tf_op jit(solution)/shard_map/psum | solution.py:77
  123.0 137.5 %copy-start.17 = (pred[16,16,16]{1,2,0:T(8,128)(4,1)}, pred[16,16,16]{1,2,0:T(8,128)(4,1)S(1)}, u32[]{:S(2)}) copy-start(pred[16,16,16]{1,2,0:T(8,128)(4,1)S(1)} %copy.351) | copy-start | bytes 12292
  214.4 1.4 copy-start.5
  217.2 31.9 %copy-start.8 = (bf16[256,2048]{0,1:T(8,128)(2,1)S(1)}, bf16[256,2048]{0,1:T(8,128)(2,1)}, u32[]{:S(2)}) copy-start(bf16[256,2048]{0,1:T(8,128)(2,1)} %get-tuple-element.49) | copy-start | bytes 3145732
  249.7 8.7 %copy-start.4 = (bf16[256,16,64,2]{0,2,3,1:T(8,128)(2,1)}, bf16[256,16,64,2]{0,2,3,1:T(8,128)(2,1)S(1)}, u32[]{:S(2)}) copy-start(bf16[256,16,64,2]{0,2,3,1:T(8,128)(2,1)S(1)} %copy.596) | copy-start | bytes 3145732
  253.5 4.9 %copy-start.10 = (bf16[16,16,8,2,128]{4,1,0,3,2:T(8,128)(2,1)S(1)}, bf16[16,16,8,2,128]{4,1,0,3,2:T(8,128)(2,1)}, u32[]{:S(2)}) copy-start(bf16[16,16,8,2,128]{4,1,0,3,2:T(8,128)(2,1)} %reshape_reshape.4) | copy-start | bytes 3145732
  260.4 1.7 copy-start.7
  260.4 1.5 copy-start.16
  260.5 2.5 copy-start.6
  263.0 1.6 copy-start.2
  263.0 1.6 copy-start.21
  266.1 81.5 %copy-start.25 = (bf16[256]{0:T(256)(128)(2,1)S(1)}, bf16[256]{0:T(256)(128)(2,1)}, u32[]{:S(2)}) copy-start(bf16[256]{0:T(256)(128)(2,1)} %param.22) | copy-start | bytes 1540
  266.2 140.2 %all-reduce.5.cloned.1.call-start = ((), (), s32[]{:S(2)}) async-start(), calls=%async_computation.8 | async-start | bytes 2097152 | tf_op jit(solution)/shard_map/psum | solution.py:77
  388.0 14.1 %copy-start.18 = (pred[16,16,16]{1,2,0:T(8,128)(4,1)S(1)}, pred[16,16,16]{1,2,0:T(8,128)(4,1)}, u32[]{:S(2)}) copy-start(pred[16,16,16]{1,2,0:T(8,128)(4,1)} %copy-done.17) | copy-start | bytes 12292
  402.0 4.3 %copy-start.3 = (bf16[16,32,8,256]{3,2,1,0:T(8,128)(2,1)}, bf16[16,32,8,256]{3,2,1,0:T(8,128)(2,1)S(1)}, u32[]{:S(2)}) copy-start(bf16[16,32,8,256]{3,2,1,0:T(8,128)(2,1)S(1)} %scatter_fusion.1) | copy-start | bytes 6291460
  (2 other events, 2.3 us)
Sparse Core Ops, SparseCore 0:
  51.6 47.1 all-gather.4
  122.9 76.5 all-gather.6
  266.3 81.2 all-reduce.2
  349.8 52.1 all-reduce.4
where the time goes:
time: 429 us; the launch traced here: 426 us
  waiting for transfers between devices  204 us (48%)
  local copies, waits for them, and re-layouts  94.6 us (22%)
  blocking collectives  49.4 us (12%)
  starting transfers between devices  31.6 us (7%)
  matrix products  20.2 us (5%)
  between operations  14.4 us (3%)
  other arithmetic  11.6 us (3%)
    psum x2, waiting for transfers between devices, by_axis(): value = lax.psum(value, axis)  81.4 us
    all_gather x1, waiting for transfers between devices, rows_first(): filled = lax.all_gather(both, axis, axis=0, tiled=True)  76.4 us
    scatter x1, local copies, waits for them, and re-layouts, per_device(): key_out = key_cache.at[seq_index, slot_index].set(key_blocks, mode='drop')  29.1 us
    all_gather x2, blocking collectives, all_in_one(): both, at, found = (lax.all_gather(jnp.concatenate(lines), axis), 0, {})  28.2 us
    all_gather x1, waiting for transfers between devices, gather_axes(): value = lax.all_gather(value, axis, axis=dim, tiled=True)  27.8 us
    unnamed x63, local copies, waits for them, and re-layouts  14.4 us
    scatter x1, local copies, waits for them, and re-layouts, per_device(): value_cache.at[seq_index, slot_index].set(value_blocks, mode='drop')  14 us
    all_gather x1, blocking collectives, gather_axes(): value = lax.all_gather(value, axis, axis=dim, tiled=True)  12.7 us
  transfers between devices with their start and end apart: 8, of which 6 were waited for; matrix products, arithmetic and copies ran while one was open for 18% of the time, Pallas kernels for 0%

commit v1 on v0

v1 whole, which is shorter than its diff:
```python
import math

import jax
import jax.numpy as jnp
from jax import lax
from jax.experimental import pallas as pl
from jax.experimental.pallas import tpu as pltpu
from jax.sharding import Mesh
from jax.sharding import PartitionSpec as P

D = 4096
KV = ("kv_0", "kv_1")
KV_TP = ("kv_0", "kv_1", "tp")
LAMBDA_SCALE = 0.2 + 0.6 * math.exp(-0.6)
NEG_FILL = -1e30

GROUPS = 4
HEADS = 8
SEQS = 4
PROPS = 16
ROWS = SEQS * PROPS
SPAN = 32
HD = 128
STAT_ROWS = 8
O_ROWS = SEQS * 2 * PROPS
O_STATS = 16


def three_terms(x):
    high = x.astype(jnp.bfloat16)
    rest = x - high.astype(jnp.float32)
    middle = rest.astype(jnp.bfloat16)
    low = (rest - middle.astype(jnp.float32)).astype(jnp.bfloat16)
    return high, middle, low


def project_kernel(tokens_ref, gain_ref, wq_ref, wk_ref, wv_ref, out_ref):
    tokens = tokens_ref[...].astype(jnp.float32)
    normed = (tokens * gain_ref[...].astype(jnp.float32)).astype(jnp.bfloat16)
    for part, ref in enumerate((wq_ref, wk_ref, wv_ref)):
        product = jnp.dot(normed, ref[...], preferred_element_type=jnp.float32)
        product = product.astype(jnp.bfloat16)
        for g in range(GROUPS):
            out_ref[g, 0, 0:ROWS, part * 256 : (part + 1) * 256] = product[
                g * ROWS : (g + 1) * ROWS
            ]
    square = tokens * tokens
    high, low, _ = three_terms(square)
    ones = jnp.ones((8, tokens.shape[1]), jnp.bfloat16)
    contract = (((1,), (1,)), ((), ()))
    power = lax.dot_general(ones, high, contract, preferred_element_type=jnp.float32)
    power = power + lax.dot_general(ones, low, contract, preferred_element_type=jnp.float32)
    terms = [t.astype(jnp.float32) for t in three_terms(power)]
    row = lax.broadcasted_iota(jnp.int32, power.shape, 0)
    zero = jnp.zeros_like(power)
    stats = jnp.where(row == 0, terms[0], zero)
    stats = jnp.where(row == 1, terms[1], stats)
    stats = jnp.where(row == 2, terms[2], stats)
    stats = stats.astype(jnp.bfloat16)
    blank = jnp.zeros((STAT_ROWS, 256), jnp.bfloat16)
    for g in range(GROUPS):
        out_ref[g, 0, ROWS : ROWS + STAT_ROWS, 0:256] = stats
        out_ref[g, 0, ROWS : ROWS + STAT_ROWS, 256:512] = blank
        out_ref[g, 0, ROWS : ROWS + STAT_ROWS, 512:768] = blank


def partial_products(tokens, gain, wq, wk, wv):
    rows, width = tokens.shape
    weight_spec = pl.BlockSpec((width, 256), lambda h: (0, h))
    return pl.pallas_call(
        project_kernel,
        grid=(HEADS,),
        in_specs=[
            pl.BlockSpec((rows, width), lambda h: (0, 0)),
            pl.BlockSpec((1, width), lambda h: (0, 0)),
            weight_spec,
            weight_spec,
            weight_spec,
        ],
        out_specs=pl.BlockSpec((GROUPS, 1, ROWS + STAT_ROWS, 768), lambda h: (0, h, 0, 0)),
        out_shape=jax.ShapeDtypeStruct((GROUPS, HEADS, ROWS + STAT_ROWS, 768), jnp.bfloat16),
        name="partial_products",
    )(tokens, gain, wq, wk, wv)


def attend_kernel(starts_ref, offset_ref, got_ref, k_ref, v_ref, o_ref, ko_ref, vo_ref):
    group = pl.program_id(0)
    offset = offset_ref[0]
    key_rows = SPAN * HEADS * 2
    cols = HEADS * 2 * PROPS
    row = lax.broadcasted_iota(jnp.int32, (key_rows, cols), 0)
    col = lax.broadcasted_iota(jnp.int32, (key_rows, cols), 1)
    same = (row % 16) == (col // PROPS)
    pair_row = lax.broadcasted_iota(jnp.int32, (SPAN * HEADS, key_rows), 0)
    pair_col = lax.broadcasted_iota(jnp.int32, (SPAN * HEADS, key_rows), 1)
    pairs = jnp.where(pair_row == pair_col // 2, 1.0, 0.0).astype(jnp.bfloat16)
    stats = []
    for s in range(SEQS):
        start = starts_ref[group * SEQS + s]
        first = start - offset
        lines = slice(s * PROPS, (s + 1) * PROPS)
        query = jnp.stack(
            [got_ref[0, :, lines, 0:HD], got_ref[0, :, lines, HD : 2 * HD]], axis=1
        ).reshape(cols, HD)
        keys = k_ref[s]
        values = v_ref[s]
        scores = lax.dot_general(
            keys, query, (((1,), (1,)), ((), ())), preferred_element_type=jnp.float32
        ) * (HD**-0.5)
        alive = same & (row < 16 * first)
        scores = jnp.where(alive, scores, NEG_FILL)
        peak = jnp.max(scores, axis=0, keepdims=True)
        weight = jnp.where(alive, jnp.exp(scores - peak), 0.0)
        total = jnp.sum(weight, axis=0, keepdims=True)
        some = total > 0.0
        safe = jnp.where(some, total, 1.0)
        weight = (weight * (1.0 / safe)).astype(jnp.bfloat16)
        level = jnp.where(some, peak + jnp.log(safe), NEG_FILL)
        stats.extend(t.astype(jnp.float32) for t in three_terms(level))
        weight = jnp.dot(pairs, weight, preferred_element_type=jnp.float32).astype(jnp.bfloat16)
        summed = lax.dot_general(
            weight, values, (((0,), (0,)), ((), ())), preferred_element_type=jnp.float32
        ).astype(jnp.bfloat16)
        for h in range(HEADS):
            o_ref[0, h, s * 32 : (s + 1) * 32, :] = summed[h * 32 : (h + 1) * 32]
        ko_ref[s] = keys
        vo_ref[s] = values

        @pl.when((first > -PROPS) & (first < SPAN))
        def _():
            lane = lax.broadcasted_iota(jnp.int32, (SPAN * HEADS, HEADS * PROPS), 1)
            line = lax.broadcasted_iota(jnp.int32, (SPAN * HEADS, HEADS * PROPS), 0)
            pick = ((line % HEADS) == (lane // PROPS)) & ((line // HEADS - first) == lane % PROPS)
            pick = jnp.where(pick, 1.0, 0.0).astype(jnp.bfloat16)
            fresh = jnp.dot(
                pick,
                got_ref[0, :, lines, 512:768].reshape(HEADS * PROPS, 256),
                preferred_element_type=jnp.float32,
            )
            at = lax.broadcasted_iota(jnp.int32, fresh.shape, 0) // HEADS - first
            inside = (at >= 0) & (at < PROPS)
            vo_ref[s] = jnp.where(inside, fresh, values.astype(jnp.float32)).astype(jnp.bfloat16)
            lane = lax.broadcasted_iota(jnp.int32, (key_rows, HEADS * PROPS), 1)
            line = lax.broadcasted_iota(jnp.int32, (key_rows, HEADS * PROPS), 0)
            here = (((line // 2) % HEADS) == (lane // PROPS)) & (
                (line // 16 - first) == lane % PROPS
            )
            fresh = jnp.zeros((key_rows, HD), jnp.float32)
            for m in range(2):
                pick = jnp.where(here & (line % 2 == m), 1.0, 0.0).astype(jnp.bfloat16)
                rows_new = got_ref[0, :, lines, 256 + m * HD : 256 + (m + 1) * HD]
                fresh = fresh + jnp.dot(
                    pick, rows_new.reshape(HEADS * PROPS, HD), preferred_element_type=jnp.float32
                )
            at = lax.broadcasted_iota(jnp.int32, fresh.shape, 0) // 16 - first
            inside = (at >= 0) & (at < PROPS)
            ko_ref[s] = jnp.where(inside, fresh, keys.astype(jnp.float32)).astype(jnp.bfloat16)

    stats.append(jnp.zeros((O_STATS - len(stats), cols), jnp.float32))
    stats = jnp.concatenate(stats, axis=0).astype(jnp.bfloat16)
    for h in range(HEADS):
        o_ref[0, h, O_ROWS : O_ROWS + O_STATS, :] = stats


def attend(starts, offset, got, keys, values):
    smem = pl.BlockSpec(memory_space=pltpu.SMEM)
    key_rows = SPAN * HEADS * 2
    return pl.pallas_call(
        attend_kernel,
        grid=(GROUPS,),
        in_specs=[
            smem,
            smem,
            pl.BlockSpec((1, HEADS, ROWS, 768), lambda g: (g, 0, 0, 0)),
            pl.BlockSpec((SEQS, key_rows, HD), lambda g: (g, 0, 0)),
            pl.BlockSpec((SEQS, SPAN * HEADS, 256), lambda g: (g, 0, 0)),
        ],
        out_specs=[
            pl.BlockSpec((1, HEADS, O_ROWS + O_STATS, 256), lambda g: (g, 0, 0, 0)),
            pl.BlockSpec((SEQS, key_rows, HD), lambda g: (g, 0, 0)),
            pl.BlockSpec((SEQS, SPAN * HEADS, 256), lambda g: (g, 0, 0)),
        ],
        out_shape=[
            jax.ShapeDtypeStruct((GROUPS, HEADS, O_ROWS + O_STATS, 256), jnp.bfloat16),
            jax.ShapeDtypeStruct(keys.shape, jnp.bfloat16),
            jax.ShapeDtypeStruct(values.shape, jnp.bfloat16),
        ],
        name="attend",
    )(starts, offset, got, keys, values)


def visible_links(parents):
    number = parents.shape[-1]
    reached = jnp.eye(number, dtype=jnp.float32) + (
        parents[..., :, None] == jnp.arange(number, dtype=jnp.int32)
    ).astype(jnp.float32)
    for _ in range(4):
        reached = jnp.minimum(jnp.einsum("bij,bjk->bik", reached, reached), 1.0)
    depths = (jnp.sum(reached, axis=-1) - 1.0).astype(jnp.int32)
    return reached > 0.5, depths


def to_all(value):
    size = lax.axis_size(KV)
    return lax.all_to_all(
        jnp.broadcast_to(value[None], (size, *value.shape)), KV, 0, 0, tiled=True
    )


def per_device(
    tokens,
    in_gain,
    query_weight,
    key_weight,
    value_weight,
    out_weight,
    lambdas,
    sub_gain,
    key_cache,
    value_cache,
    cache_len,
    accepted,
    parents,
):
    seq_count, prop_count, width_part = tokens.shape
    row_count = seq_count * prop_count
    me = lax.axis_index(KV)
    group = me // HEADS
    head = me % HEADS
    starts = cache_len + accepted
    partial = partial_products(
        tokens.reshape(row_count, width_part),
        in_gain.reshape(1, width_part),
        query_weight,
        key_weight,
        value_weight,
    )
    arrived = lax.all_to_all(
        partial.reshape(GROUPS * HEADS, ROWS + STAT_ROWS, 768), KV, 0, 0, tiled=True
    )
    summed = jnp.sum(arrived.astype(jnp.float32), axis=0)
    power = jnp.sum(summed[ROWS : ROWS + 3, 0:256], axis=0)
    power = lax.dynamic_slice(power, (group * ROWS,), (ROWS,))
    row_scale = lax.rsqrt(power / D + 1e-06)
    scaled = summed[:ROWS] * row_scale[:, None]
    own_starts = lax.dynamic_slice(starts, (group * SEQS,), (SEQS,))
    own_parents = lax.dynamic_slice(parents, (group * SEQS, 0), (SEQS, prop_count))
    visible, depths = visible_links(own_parents)
    positions = (own_starts[:, None] + depths).reshape(ROWS)
    half_dim = HD // 2
    frequency = 10000.0 ** (-jnp.arange(half_dim, dtype=jnp.float32) / half_dim)
    angles = positions.astype(jnp.float32)[:, None] * frequency[None, :]
    cosine = jnp.cos(angles)[:, None]
    sine = jnp.sin(angles)[:, None]
    vectors = scaled[:, :512].reshape(ROWS, 4, HD)
    lower = vectors[..., :half_dim]
    upper = vectors[..., half_dim:]
    turned = jnp.concatenate(
        [lower * cosine - upper * sine, upper * cosine + lower * sine], axis=-1
    ).reshape(ROWS, 512)
    own = jnp.concatenate([turned, scaled[:, 512:]], axis=1).astype(jnp.bfloat16)
    got = to_all(own).reshape(GROUPS, HEADS, ROWS, 768)
    offset = (me * SPAN).astype(jnp.int32).reshape(1)
    parts, key_out, value_out = attend(
        starts,
        offset,
        got,
        key_cache.reshape(seq_count, SPAN * HEADS * 2, HD),
        value_cache.reshape(seq_count, SPAN * HEADS, 256),
    )
    merged = lax.all_to_all(
        parts.reshape(GROUPS * HEADS, O_ROWS + O_STATS, 256), KV, 0, 0, tiled=True
    )
    levels = merged[:, O_ROWS : O_ROWS + 3 * SEQS].astype(jnp.float32)
    levels = lax.dynamic_slice(levels, (0, 0, head * 32), (32, 3 * SEQS, 32))
    levels = jnp.sum(levels.reshape(32, SEQS, 3, 32), axis=2).reshape(32, SEQS, 2, PROPS)
    own_blocks = own.reshape(SEQS, PROPS, 6, HD)
    own_scores = jnp.einsum(
        "sqmd,sjmd->smqj",
        own_blocks[:, :, 0:2],
        own_blocks[:, :, 2:4],
        preferred_element_type=jnp.float32,
    ) * (HD**-0.5)
    seen = visible[:, None]
    own_scores = jnp.where(seen, own_scores, NEG_FILL)
    peak = jnp.maximum(jnp.max(own_scores, axis=-1), jnp.max(levels, axis=0))
    own_weight = jnp.where(seen, jnp.exp(own_scores - peak[..., None]), 0.0)
    share = jnp.exp(levels - peak[None])
    total = jnp.sum(own_weight, axis=-1) + jnp.sum(share, axis=0)
    lam = lax.dynamic_slice(lambdas, (head,), (1,))
    sign = jnp.concatenate([jnp.ones((1,), jnp.float32), -lam])[None, :, None] / total
    share = share * sign[None]
    own_weight = own_weight * sign[..., None]
    own_mix = jnp.sum(own_weight, axis=1).astype(jnp.bfloat16)
    own_values = own[:, 512:].reshape(SEQS, PROPS, 256)
    attended = jnp.sum(
        merged[:, :O_ROWS].astype(jnp.float32).reshape(32, SEQS, 2, PROPS, 256)
        * share[..., None],
        axis=(0, 2),
    )
    attended = attended + jnp.einsum(
        "sqj,sje->sqe", own_mix, own_values, preferred_element_type=jnp.float32
    )
    mixed = attended * lax.rsqrt(jnp.mean(attended * attended, axis=-1, keepdims=True) + 1e-05)
    mixed = (mixed * sub_gain.astype(jnp.float32) * LAMBDA_SCALE).astype(jnp.bfloat16)
    mixed_all = to_all(mixed.reshape(ROWS, 256)).reshape(GROUPS, HEADS, ROWS, 256)
    product = jnp.einsum(
        "ghre,hec->grc",
        mixed_all,
        out_weight.reshape(HEADS, 256, -1),
        preferred_element_type=jnp.float32,
    ).astype(jnp.bfloat16)
    halves = jnp.moveaxis(product.reshape(row_count, 2, -1), 1, 0)
    both = lax.all_to_all(halves, "tp", 0, 0, tiled=True).astype(jnp.float32)
    output = (both[0] + both[1]).astype(jnp.bfloat16).reshape(seq_count, prop_count, -1)
    return (output, key_out.reshape(key_cache.shape), value_out.reshape(value_cache.shape))


def solution(mesh):
    torus = Mesh(
        mesh.devices.reshape(mesh.shape["dp"], 8, 4, mesh.shape["tp"]), ("dp", "kv_0", "kv_1", "tp")
    )
    placed = (
        P("dp", None, KV),
        P(KV),
        P(KV, "tp"),
        P(KV, "tp"),
        P(KV, "tp"),
        P("tp", KV),
        P("tp"),
        P(),
        P("dp", KV, "tp", None, None),
        P("dp", KV, "tp", None),
        P("dp"),
        P("dp"),
        P("dp", None),
    )
    return jax.shard_map(
        per_device,
        mesh=torus,
        in_specs=placed,
        out_specs=(P("dp", None, KV_TP), P("dp", KV, "tp", None, None), P("dp", KV, "tp", None)),
        check_vma=False,
    )
```

time: 429 us -> 307 us (0.72)
  local copies, waits for them, and re-layouts: 94.6 us -> 5.32 us
  Pallas kernels: 0 us -> 24.2 us
  matrix products: 20.2 us -> 1.52 us
  between operations: 14.4 us -> 1.73 us
  blocking collectives: 49.4 us -> 39.2 us
  other arithmetic: 11.6 us -> 5.17 us
  waiting for transfers between devices: 204 us -> 199 us
    all_to_all x4 -> x3, waiting for transfers between devices: 18.3 us -> 199 us  [the longest x1 76.6 us: per_device(): lax.all_to_all(partial.reshape(GROUPS * HEADS, ROWS + STAT_ROWS, 768), KV...]
    all_gather x2 -> x0, waiting for transfers between devices: 104 us -> none  [the longest x1 76.4 us: rows_first(): filled = lax.all_gather(both, axis, axis=0, tiled=True)]
    psum x2 -> x0, waiting for transfers between devices: 81.4 us -> none  [by_axis(): value = lax.psum(value, axis)]
    scatter x2 -> x0, local copies, waits for them, and re-layouts: 43.2 us -> none  [the longest x1 29.1 us: per_device(): key_out = key_cache.at[seq_index, slot_index].set(key_blocks, mode='drop')]
    all_gather x3 -> x0, blocking collectives: 40.9 us -> none  [the longest x2 28.2 us: all_in_one(): both, at, found = (lax.all_gather(jnp.concatenate(lines), axis), 0, {})]
    all_to_all x1 -> x2, blocking collectives: 8.56 us -> 39.2 us  [the longest x1 32.9 us: to_all(): lax.all_to_all(jnp.broadcast_to(value[None], (size, *value.shape)), KV, 0...]
    pallas_call x0 -> x2, Pallas kernels: none -> 24.2 us  [the longest x1 17.3 us: attend(): pl.pallas_call(attend_kernel, grid=(GROUPS,), in_specs=[smem, smem, pl.Bl...]
    dot_general x24 -> x5, matrix products: 20.2 us -> 1.52 us  [the longest x2 0.66 us: visible_links(): reached = jnp.minimum(jnp.einsum('bij,bjk->bik', reached, reached), 1.0)]
  transfers between devices with their start and end apart: 8 -> 3, of which waited for: 6 -> 3; matrix products, arithmetic and copies ran while one was open for 18% -> 1% of each run, Pallas kernels for 0% -> 0%
where the time goes in v1:
time: 307 us; the launch traced here: 306 us
  waiting for transfers between devices  199 us (65%)
  blocking collectives  39.2 us (13%)
  starting transfers between devices  30.2 us (10%)
  Pallas kernels  24.2 us (8%)
  local copies, waits for them, and re-layouts  5.32 us (2%)
  other arithmetic  5.17 us (2%)
    all_to_all x1, waiting for transfers between devices, per_device(): lax.all_to_all(partial.reshape(GROUPS * HEADS, ROWS + STAT_ROWS, 768), KV...  76.6 us
    all_to_all x1, waiting for transfers between devices, to_all(): lax.all_to_all(jnp.broadcast_to(value[None], (size, *value.shape)), KV, 0...  70.3 us
    all_to_all x1, waiting for transfers between devices, per_device(): lax.all_to_all(parts.reshape(GROUPS * HEADS, O_ROWS + O_STATS, 256), KV,...  51.7 us
    all_to_all x1, blocking collectives, to_all(): lax.all_to_all(jnp.broadcast_to(value[None], (size, *value.shape)), KV, 0...  32.9 us
    pallas_call x1, Pallas kernels, attend(): pl.pallas_call(attend_kernel, grid=(GROUPS,), in_specs=[smem, smem, pl.Bl...  17.3 us
    all_to_all x1, starting transfers between devices, per_device(): lax.all_to_all(partial.reshape(GROUPS * HEADS, ROWS + STAT_ROWS, 768), KV...  12.3 us
    all_to_all x1, starting transfers between devices, per_device(): lax.all_to_all(parts.reshape(GROUPS * HEADS, O_ROWS + O_STATS, 256), KV,...  9.23 us
    all_to_all x1, starting transfers between devices, to_all(): lax.all_to_all(jnp.broadcast_to(value[None], (size, *value.shape)), KV, 0...  8.67 us
  transfers between devices with their start and end apart: 3, of which 3 were waited for; matrix products, arithmetic and copies ran while one was open for 1% of the time, Pallas kernels for 0%

profile of v1, /device:TPU:1, one launch (start us, length us, event | category | flops | bytes accessed | tf_op | source)
XLA Modules:
  0.0 305.9 jit_solution(16516103642675117745)
XLA Ops:
  0.6 6.9 %partial_products.1 = bf16[4,8,72,768]{3,2,1,0:T(8,128)(2,1)} custom-call(bf16[256,128]{1,0:T(8,128)(2,1)} %bitcast.48, bf16[1,128]{1,0:T(2,128)(2,1)} %bitcast.50, bf16[128,2048]{1,0:T(8,128)(2,1)} %wq_ref.1, bf16[128,2048]{1,0:T(8,128)(2,1)} %wk_ref.1, bf16[128,2048]{1,0:T(8,128)(2,1)} %wv_ref.1), custom_call_target="tpu_custom_call" | custom-call | tf_op jit(solution)/shard_map/partial_products/pallas_call | solution.py:70
  7.5 12.3 %all-to-all-start = ((bf16[32,72,768]{2,1,0:T(8,128)(2,1)}), bf16[32,72,768]{2,1,0:T(8,128)(2,1)}, u32[]{:S(2)}, u32[]{:S(2)}) async-start(bf16[32,72,768]{2,1,0:T(8,128)(2,1)} %bitcast.36), calls=%async_computation | async-start | bytes 7077888 | tf_op jit(solution)/shard_map/all_to_all | solution.py:238
  20.0 0.7 constant_dynamic-slice_fusion.1
  20.7 0.3 convolution_minimum_fusion.2
  21.0 0.3 fusion.21
  21.5 0.2 multiply_cosine_fusion
  21.7 76.6 %all-to-all-done = bf16[32,72,768]{2,1,0:T(8,128)(2,1)} async-done(((bf16[32,72,768]{2,1,0:T(8,128)(2,1)}), bf16[32,72,768]{2,1,0:T(8,128)(2,1)}, u32[]{:S(2)}, u32[]{:S(2)}) %all-to-all-start) | async-done | bytes 3538976 | tf_op jit(solution)/shard_map/all_to_all | solution.py:238
  98.3 2.5 convert_reduce_fusion
  101.1 0.2 multiply_subtract_fusion
  101.3 0.1 pad_maximum_fusion
  101.5 2.1 broadcast_in_dim.24
  103.5 8.7 %all-to-all-start.1 = ((bf16[32,64,768]{2,1,0:T(8,128)(2,1)}), bf16[32,64,768]{2,1,0:T(8,128)(2,1)}, u32[]{:S(2)}, u32[]{:S(2)}) async-start(bf16[32,64,768]{2,1,0:T(8,128)(2,1)} %broadcast_in_dim.24), calls=%async_computation.1 | async-start | bytes 6291456 | tf_op jit(solution)/shard_map/all_to_all | solution.py:205
  112.2 70.3 %all-to-all-done.1 = bf16[32,64,768]{2,1,0:T(8,128)(2,1)} async-done(((bf16[32,64,768]{2,1,0:T(8,128)(2,1)}), bf16[32,64,768]{2,1,0:T(8,128)(2,1)}, u32[]{:S(2)}, u32[]{:S(2)}) %all-to-all-start.1) | async-done | bytes 3145760 | tf_op jit(solution)/shard_map/all_to_all | solution.py:205
  182.5 17.3 %attend.1 = (bf16[4,8,144,256]{3,2,1,0:T(8,128)(2,1)}, bf16[16,512,128]{2,1,0:T(8,128)(2,1)}, bf16[16,256,256]{2,1,0:T(8,128)(2,1)}) custom-call(s32[16]{0:T(128)} %copy-done.2, s32[1]{0:T(128)} %bitcast.offset_ref, bf16[4,8,64,768]{3,2,1,0:T(8,128)(2,1)} %bitcast.4.got_ref, bf16[16,512,128]{2,1,0:T(8,128)(2,1)} %bitcast.39, bf16[16,256,256]{2,1,0:T(8,128)(2,1)} %bitcast.40), custom_call_target="tpu_custom_call" | custom-call | tf_op jit(solution)/shard_map/attend/pallas_call | solution.py:168
  199.8 9.2 %all-to-all-start.2 = ((bf16[32,144,256]{2,1,0:T(8,128)(2,1)}), bf16[32,144,256]{2,1,0:T(8,128)(2,1)S(1)}, u32[]{:S(2)}, u32[]{:S(2)}) async-start(bf16[32,144,256]{2,1,0:T(8,128)(2,1)} %bitcast.38), calls=%async_computation.2 | async-start | bytes 4718592 | tf_op jit(solution)/shard_map/all_to_all | solution.py:271
  209.1 0.6 dynamic_slice.19
  210.7 0.1 convert_element_type.80
  210.9 0.2 fusion.22
  211.2 51.7 %all-to-all-done.2 = bf16[32,144,256]{2,1,0:T(8,128)(2,1)S(1)} async-done(((bf16[32,144,256]{2,1,0:T(8,128)(2,1)}), bf16[32,144,256]{2,1,0:T(8,128)(2,1)S(1)}, u32[]{:S(2)}, u32[]{:S(2)}) %all-to-all-start.2) | async-done | bytes 2359328 | tf_op jit(solution)/shard_map/all_to_all | solution.py:271
  263.0 0.1 constant_dynamic-slice_fusion
  263.6 0.1 reshape.245
  264.0 0.7 multiply_reduce_fusion
  264.8 0.3 multiply_reduce_fusion.1
  265.0 0.1 multiply_convert_fusion
  265.1 0.1 broadcast_in_dim.29
  265.3 32.9 %all_to_all.25 = bf16[32,64,256]{2,1,0:T(8,128)(2,1)S(1)} all-to-all(bf16[32,64,256]{2,1,0:T(8,128)(2,1)S(1)} %broadcast_in_dim.29), channel_id=1, replica_groups=mesh['dp'=4,'kv_0'=8,'kv_1'=4,'tp'=2] {'kv_0','kv_1'}, dimensions={0} | all-to-all | bytes 2097152 | tf_op jit(solution)/shard_map/all_to_all | solution.py:205
  298.2 0.4 fusion
  298.6 0.1 reshape.249
  298.7 0.1 copy.48
  298.8 6.3 %all_to_all.26 = bf16[2,256,64]{1,2,0:T(8,128)(2,1)S(1)} all-to-all(bf16[2,256,64]{1,2,0:T(8,128)(2,1)S(1)} %copy.48), channel_id=1, replica_groups=mesh['dp'=4,'kv_0'=8,'kv_1'=4,'tp'=2] {'tp'}, dimensions={0} | all-to-all | bytes 131072 | tf_op jit(solution)/shard_map/all_to_all | solution.py:314
  305.1 0.1 copy.49
  305.3 0.6 fusion.2
  (61 shorter events, 1.9 us)
Async XLA Ops:
  0.6 297.5 %copy-start = (bf16[2048,128]{1,0:T(8,128)(2,1)S(1)}, bf16[2048,128]{1,0:T(8,128)(2,1)}, u32[]{:S(2)}) copy-start(bf16[2048,128]{1,0:T(8,128)(2,1)} %param.18) | copy-start | bytes 1572868
  7.5 12.3 %copy-start.3 = (s32[16]{0:T(128)S(1)}, s32[16]{0:T(128)}, u32[]{:S(2)}) copy-start(s32[16]{0:T(128)} %param.23) | copy-start | bytes 196
  7.5 12.3 %copy-start.4 = (s32[16]{0:T(128)S(1)}, s32[16]{0:T(128)}, u32[]{:S(2)}) copy-start(s32[16]{0:T(128)} %param.24) | copy-start | bytes 196
  7.5 90.8 %all-to-all-start = ((bf16[32,72,768]{2,1,0:T(8,128)(2,1)}), bf16[32,72,768]{2,1,0:T(8,128)(2,1)}, u32[]{:S(2)}, u32[]{:S(2)}) async-start(bf16[32,72,768]{2,1,0:T(8,128)(2,1)} %bitcast.36), calls=%async_computation | async-start | bytes 7077888 | tf_op jit(solution)/shard_map/all_to_all | solution.py:238
  19.9 83.7 %copy-start.2 = (s32[16]{0:T(128)}, s32[16]{0:T(128)S(1)}, u32[]{:S(2)}) copy-start(s32[16]{0:T(128)S(1)} %add.95.starts_ref) | copy-start | bytes 196
  101.5 109.2 %copy-start.1 = (bf16[64,768]{1,0:T(8,128)(2,1)}, bf16[64,768]{1,0:T(8,128)(2,1)S(1)}, u32[]{:S(2)}) copy-start(bf16[64,768]{1,0:T(8,128)(2,1)S(1)} %maximum_convert_fusion) | copy-start | bytes 294916
  103.5 78.9 %all-to-all-start.1 = ((bf16[32,64,768]{2,1,0:T(8,128)(2,1)}), bf16[32,64,768]{2,1,0:T(8,128)(2,1)}, u32[]{:S(2)}, u32[]{:S(2)}) async-start(bf16[32,64,768]{2,1,0:T(8,128)(2,1)} %broadcast_in_dim.24), calls=%async_computation.1 | async-start | bytes 6291456 | tf_op jit(solution)/shard_map/all_to_all | solution.py:205
  199.8 9.3 %copy-start.5 = (f32[8]{0:T(128)S(1)}, f32[8]{0:T(128)}, u32[]{:S(2)}) copy-start(f32[8]{0:T(128)} %param.19) | copy-start | bytes 100
  199.8 10.5 %copy-start.6 = (bf16[256]{0:T(256)(128)(2,1)S(1)}, bf16[256]{0:T(256)(128)(2,1)}, u32[]{:S(2)}) copy-start(bf16[256]{0:T(256)(128)(2,1)} %param.20) | copy-start | bytes 1540
  199.8 63.2 %all-to-all-start.2 = ((bf16[32,144,256]{2,1,0:T(8,128)(2,1)}), bf16[32,144,256]{2,1,0:T(8,128)(2,1)S(1)}, u32[]{:S(2)}, u32[]{:S(2)}) async-start(bf16[32,144,256]{2,1,0:T(8,128)(2,1)} %bitcast.38), calls=%async_computation.2 | async-start | bytes 4718592 | tf_op jit(solution)/shard_map/all_to_all | solution.py:271
  210.8 53.9 %slice-start = ((bf16[64,768]{1,0:T(8,128)(2,1)}), bf16[64,256]{1,0:T(8,128)(2,1)S(1)}, s32[]{:S(2)}) async-start(bf16[64,768]{1,0:T(8,128)(2,1)} %copy-done.1), calls=%async_computation.5 | async-start | bytes 65536 | tf_op jit(solution)/shard_map/slice | solution.py:295
